TPU v7x, 512 devices: a whole 4x4x16 slice. The times are simulated.
512 devices in a mesh: ep: 32 (over z, core), tp: 16 (over y, x).
Axes of the slice: x: 4, y: 4, z: 16, core: 2. Of those that a mesh axis runs over, the one named last changes fastest.
Arguments:
- tokens: bfloat16 [8192, 2048], P('ep', 'tp'), may hold values from -800 to 800
- norm_gain: bfloat16 [2048], P('tp'), may hold values from 0.099609375 to 1.8984375
- w_gate: bfloat16 [32, 2048, 6144], P('ep', None, 'tp'), may hold values from -0.125 to 0.125
- w_up: bfloat16 [32, 2048, 6144], P('ep', None, 'tp'), may hold values from -0.125 to 0.125
- w_down: bfloat16 [32, 6144, 2048], P('ep', 'tp'), may hold values from -1.2757759 to 1.2757759
- routes: int32 [8192, 2], P('ep'), may hold values from 0 to 31, all different within a row; in each aligned block of 256 rows (0 to 255, 256 to 511, ...) at most 32 rows name the same one
- route_weights: float32 [8192, 2], P('ep'), may hold values from 0.1 to 1
- final_gain: bfloat16 [2048], P('tp'), may hold values from 0.099609375 to 1.8984375
Outputs:
- mixed_out: bfloat16 [8192, 2048], P('ep', 'tp')
Inputs may be any that keep to these rules, and one draw needn't show every extreme that they name: `routes`: A token's 2 experts differ. Among the tokens of one index of ep (aligned blocks of 256 rows), no expert is named by more than 32 tokens, a bound that some block reaches.
All inputs are finite; a program needn't handle non-finite values.
Results may differ from a plain program's by a relative error of at most 0.017.
Values may be sent and summed in bfloat16 or wider, within the bound.
A program may use at most 64 MiB of HBM per device.

v0:
```python
import jax
import jax.numpy as jnp
from jax import lax
from jax.sharding import PartitionSpec as P

EPS = 1e-06


def from_everyone(shard, axis):
    copies = jnp.broadcast_to(shard, (lax.axis_size(axis), *shard.shape))
    return lax.all_to_all(copies, axis, split_axis=0, concat_axis=0, tiled=True)


def over_copies(shard, axis):
    return from_everyone(shard, axis).sum(axis=0)


def cut_along(shard, dim, length):
    before, after = (shard.shape[:dim], shard.shape[dim + 1 :])
    return jnp.moveaxis(shard.reshape(*before, length, -1, *after), dim, 0)


def summed_on_arrival(shard, axis, dim):
    length = lax.axis_size(axis)
    tiles = lax.all_to_all(cut_along(shard, dim, length), axis, 0, 0, tiled=True)
    return jnp.sum(tiles.astype(jnp.float32), axis=0)


def slot_targets(routes, experts, capacity):
    flat = routes.reshape(-1)
    onehot = (flat[:, None] == jnp.arange(experts, dtype=jnp.int32)[None, :]).astype(jnp.int32)
    before = jnp.cumsum(onehot, axis=0) - onehot
    slot = jnp.sum(before * onehot, axis=1)
    return flat * capacity + slot


def local(tokens, norm_gain, w_gate, w_up, w_down, routes, route_weights, final_gain):
    experts = lax.axis_size("ep")
    tok_rows = tokens.shape[0]
    share = tokens.shape[1]
    width = share * lax.axis_size("tp")
    topk = routes.shape[1]
    capacity = 2 * tok_rows * topk // experts
    wide = tokens.astype(jnp.float32)
    input_squares = over_copies(jnp.sum(wide * wide, axis=1), "tp")
    scale = lax.rsqrt(input_squares / width + EPS)
    normed = (wide * scale[:, None] * norm_gain.astype(jnp.float32)[None, :]).astype(jnp.bfloat16)
    target = slot_targets(routes, experts, capacity)
    sources = jnp.repeat(jnp.arange(tok_rows, dtype=jnp.int32), topk)
    gate_w = w_gate[0]
    up_w = w_up[0]
    down_w = w_down[0]
    outbox = jnp.zeros((experts * capacity, share), jnp.bfloat16).at[target].set(normed[sources])
    inbox = lax.all_to_all(outbox, "ep", split_axis=0, concat_axis=0, tiled=True)
    piece = lax.all_gather(inbox, "tp", axis=1, tiled=True)
    gate = jnp.dot(piece, gate_w, preferred_element_type=jnp.float32)
    up = jnp.dot(piece, up_w, preferred_element_type=jnp.float32)
    hidden = (jax.nn.silu(gate) * up).astype(jnp.bfloat16)
    sums = summed_on_arrival(
        lax.dot_general(
            down_w, hidden, (((0,), (1,)), ((), ())), preferred_element_type=jnp.float32
        ).astype(jnp.bfloat16),
        "tp",
        0,
    )
    returned = lax.all_to_all(
        sums.astype(jnp.bfloat16), "ep", split_axis=1, concat_axis=1, tiled=True
    )
    picked = jnp.take(returned, target, axis=1).reshape(returned.shape[0], tok_rows, topk)
    combined = jnp.einsum("dtk,tk->td", picked.astype(jnp.float32), route_weights)
    local_squares = jnp.sum(combined * combined, axis=1)
    total_squares = over_copies(local_squares, "tp")
    final_scale = lax.rsqrt(total_squares / width + EPS)
    return (combined * final_scale[:, None] * final_gain.astype(jnp.float32)[None, :]).astype(
        jnp.bfloat16
    )


def solution(mesh):
    in_specs = (
        P("ep", "tp"),
        P("tp"),
        P("ep", None, "tp"),
        P("ep", None, "tp"),
        P("ep", "tp", None),
        P("ep", None),
        P("ep", None),
        P("tp"),
    )
    out_specs = P("ep", "tp")
    return jax.shard_map(local, mesh=mesh, in_specs=in_specs, out_specs=out_specs, check_vma=False)
```

profile of v0, /device:TPU:1, one launch (start us, length us, event | category | flops | bytes accessed | tf_op | source)
XLA Modules:
  0.0 259.8 jit_solution(18186526171175588482)
XLA Ops:
  6.5 1.1 fusion.9
  7.6 0.6 broadcast_in_dim.31
  8.3 7.6 %all-to-all-start = ((f32[16,1,256]{2,1,0:T(1,128)}), f32[16,1,256]{2,1,0:T(1,128)S(1)}, u32[]{:S(2)}, u32[]{:S(2)}) async-start(f32[16,1,256]{2,1,0:T(1,128)} %broadcast_in_dim.31), calls=%async_computation | async-start | bytes 32768 | tf_op jit(solution)/shard_map/all_to_all | solution.py:11
  15.9 0.8 copy.31
  17.0 0.7 broadcast_multiply_fusion
  17.7 1.2 reduce-window.6
  19.7 0.7 convert_element_type.37
  20.4 1.9 all-to-all-done
  22.3 0.9 fusion.11
  23.3 3.1 %scatter_custom_fusion = bf16[1024,128]{1,0:T(8,128)(2,1)S(1)} fusion(s32[512]{0:T(512)S(1)} %bitcast.62, bf16[256,128]{1,0:T(8,128)(2,1)S(1)} %fusion.11, s32[1024]{0:T(1024)S(1)} %pad_clamp_fusion.1, bf16[]{:T(256)} %constant.34.clone.1), kind=kCustom, calls=%fused_computation.17 | custom fusion | bytes 262146 | tf_op jit(solution)/shard_map/scatter | solution.py:53
  26.3 39.5 %all_to_all.41 = bf16[32,32,128]{2,1,0:T(8,128)(2,1)} all-to-all(bf16[32,32,128]{2,1,0:T(8,128)(2,1)S(1)} %bitcast.57), channel_id=1, replica_groups=mesh['ep'=32,'tp'=16] {'ep'}, dimensions={0} | all-to-all | bytes 524288 | tf_op jit(solution)/shard_map/all_to_all | solution.py:54
  65.9 59.4 %all-gather.2.cloned.1.call-done = bf16[1024,2048]{1,0:T(8,128)(2,1)} async-done(((bf16[1024,128]{1,0:T(8,128)(2,1)}), bf16[1024,2048]{1,0:T(8,128)(2,1)}) %all-gather.2.cloned.1.call-update) | async-done | bytes 4194320 | tf_op jit(solution)/shard_map/all_gather | solution.py:55
  125.3 5.7 %fusion.3 = f32[1024,384]{1,0:T(8,128)} fusion(bf16[1024,2048]{1,0:T(8,128)(2,1)} %all-gather.2.cloned.1.call-done, bf16[1,2048,384]{2,1,0:T(8,128)(2,1)S(1)} %copy-done.3), kind=kOutput, calls=%fused_computation.8 | convolution fusion | flops 1610612736 | bytes 7340032 | tf_op jit(solution)/shard_map/dot_general | solution.py:56
  131.0 9.6 %convert_bitcast_fusion = bf16[128,16,8,128]{3,2,1,0:T(8,128)(2,1)} fusion(bf16[1,384,2048]{2,1,0:T(8,128)(2,1)S(1)} %copy-done, f32[1024,384]{1,0:T(8,128)} %fusion.3, bf16[1024,2048]{1,0:T(8,128)(2,1)} %all-gather.2.cloned.1.call-done, bf16[1,2048,384]{2,1,0:T(8,128)(2,1)} %param.11), kind=kOutput, calls=%fused_computation.4 | convolution fusion | flops 3225681920 | bytes 13107200 | tf_op jit(solution)/shard_map/dot_general | solution.py:60
  140.6 3.3 %copy.48 = bf16[128,16,8,128]{3,2,0,1:T(8,128)(2,1)S(1)} copy(bf16[128,16,8,128]{3,2,1,0:T(8,128)(2,1)} %convert_bitcast_fusion) | data formatting | bytes 8388608 | tf_op jit(solution)/shard_map/reshape | solution.py:20
  143.9 54.5 %all_to_all.42 = bf16[16,128,1024]{1,2,0:T(8,128)(2,1)} all-to-all(bf16[16,128,1024]{1,2,0:T(8,128)(2,1)S(1)} %bitcast.54), channel_id=1, replica_groups=mesh['ep'=32,'tp'=16] {'tp'}, dimensions={0} | all-to-all | bytes 8388608 | tf_op jit(solution)/shard_map/all_to_all | solution.py:25
  198.3 3.5 %reduce_sum.66 = bf16[128,1024]{0,1:T(8,128)(2,1)} reduce(bf16[16,128,1024]{1,2,0:T(8,128)(2,1)} %all_to_all.42, bf16[]{:T(256)} %constant.34.clone.1), dimensions={0}, to_apply=%region_6.7 | reduce | flops 1966080 | bytes 4456450 | tf_op jit(solution)/shard_map/reduce_sum | solution.py:26
  201.9 15.5 %all-to-all-start.3 = ((bf16[128,32,32]{0,2,1:T(8,128)(2,1)}), bf16[128,32,32]{0,2,1:T(8,128)(2,1)S(1)}, u32[]{:S(2)}, u32[]{:S(2)}) async-start(bf16[128,32,32]{0,2,1:T(8,128)(2,1)} %bitcast.10), calls=%async_computation.3 | async-start | bytes 524288 | tf_op jit(solution)/shard_map/all_to_all | solution.py:66
  218.0 21.6 %all-to-all-done.3 = bf16[128,32,32]{0,2,1:T(8,128)(2,1)S(1)} async-done(((bf16[128,32,32]{0,2,1:T(8,128)(2,1)}), bf16[128,32,32]{0,2,1:T(8,128)(2,1)S(1)}, u32[]{:S(2)}, u32[]{:S(2)}) %all-to-all-start.3) | async-done | bytes 262176 | tf_op jit(solution)/shard_map/all_to_all | solution.py:66
  239.7 1.3 gather_fusion
  241.6 0.6 broadcast_in_dim.34
  242.2 3.5 %all-to-all-start.4 = ((f32[16,1,256]{2,1,0:T(1,128)}), f32[16,1,256]{2,1,0:T(1,128)S(1)}, u32[]{:S(2)}, u32[]{:S(2)}) async-start(f32[16,1,256]{2,1,0:T(1,128)} %broadcast_in_dim.34), calls=%async_computation.4 | async-start | bytes 32768 | tf_op jit(solution)/shard_map/all_to_all | solution.py:11
  245.8 6.4 %all-to-all-done.4 = f32[16,1,256]{2,1,0:T(1,128)S(1)} async-done(((f32[16,1,256]{2,1,0:T(1,128)}), f32[16,1,256]{2,1,0:T(1,128)S(1)}, u32[]{:S(2)}, u32[]{:S(2)}) %all-to-all-start.4) | async-done | bytes 16416 | tf_op jit(solution)/shard_map/all_to_all | solution.py:11
  252.2 0.7 multiply_convert_fusion.1
  (39 shorter events, 2.5 us)
Async XLA Ops:
  6.5 124.5 %copy-start = (bf16[1,384,2048]{2,1,0:T(8,128)(2,1)S(1)}, bf16[1,384,2048]{2,1,0:T(8,128)(2,1)}, u32[]{:S(2)}) copy-start(bf16[1,384,2048]{2,1,0:T(8,128)(2,1)} %param.12) | copy-start | bytes 4718596
  6.5 118.7 %copy-start.3 = (bf16[1,2048,384]{2,1,0:T(8,128)(2,1)S(1)}, bf16[1,2048,384]{2,1,0:T(8,128)(2,1)}, u32[]{:S(2)}) copy-start(bf16[1,2048,384]{2,1,0:T(8,128)(2,1)} %param.10) | copy-start | bytes 4718596
  8.3 14.0 %all-to-all-start = ((f32[16,1,256]{2,1,0:T(1,128)}), f32[16,1,256]{2,1,0:T(1,128)S(1)}, u32[]{:S(2)}, u32[]{:S(2)}) async-start(f32[16,1,256]{2,1,0:T(1,128)} %broadcast_in_dim.31), calls=%async_computation | async-start | bytes 32768 | tf_op jit(solution)/shard_map/all_to_all | solution.py:11
  15.8 109.4 %all-gather.2.cloned.1.call-start = ((), (), s32[]{:S(2)}) async-start(), calls=%async_computation.5 | async-start | bytes 4456448 | tf_op jit(solution)/shard_map/all_gather | solution.py:55
  198.3 19.3 %copy-start.1 = (s32[256,2]{0,1:T(2,128)S(1)}, s32[256,2]{0,1:T(2,128)}, u32[]{:S(2)}) copy-start(s32[256,2]{0,1:T(2,128)} %param.13) | copy-start | bytes 6148
  198.3 19.5 %copy-start.2 = (f32[256,2]{0,1:T(2,128)S(1)}, f32[256,2]{0,1:T(2,128)}, u32[]{:S(2)}) copy-start(f32[256,2]{0,1:T(2,128)} %param.14) | copy-start | bytes 6148
  201.9 37.8 %all-to-all-start.3 = ((bf16[128,32,32]{0,2,1:T(8,128)(2,1)}), bf16[128,32,32]{0,2,1:T(8,128)(2,1)S(1)}, u32[]{:S(2)}, u32[]{:S(2)}) async-start(bf16[128,32,32]{0,2,1:T(8,128)(2,1)} %bitcast.10), calls=%async_computation.3 | async-start | bytes 524288 | tf_op jit(solution)/shard_map/all_to_all | solution.py:66
  239.7 6.1 %copy-start.4 = (bf16[128]{0:T(256)(128)(2,1)S(1)}, bf16[128]{0:T(256)(128)(2,1)}, u32[]{:S(2)}) copy-start(bf16[128]{0:T(256)(128)(2,1)} %param.15) | copy-start | bytes 772
  242.2 9.9 %all-to-all-start.4 = ((f32[16,1,256]{2,1,0:T(1,128)}), f32[16,1,256]{2,1,0:T(1,128)S(1)}, u32[]{:S(2)}, u32[]{:S(2)}) async-start(f32[16,1,256]{2,1,0:T(1,128)} %broadcast_in_dim.34), calls=%async_computation.4 | async-start | bytes 32768 | tf_op jit(solution)/shard_map/all_to_all | solution.py:11
Sparse Core Ops, SparseCore 0:
  66.0 59.2 all-gather.1
where the time goes:
time: 260 us
  blocking collectives  94 us (36%)
  waiting for transfers between devices  89.3 us (34%)
  starting transfers between devices  26.6 us (10%)
  matrix products  15.8 us (6%)
  between operations  13.6 us (5%)
  local copies, waits for them, and re-layouts  11.2 us (4%)
  other arithmetic  9.22 us (4%)
    all_gather x1, waiting for transfers between devices, local(): piece = lax.all_gather(inbox, 'tp', axis=1, tiled=True)  59.4 us
    all_to_all x1, blocking collectives, summed_on_arrival(): lax.all_to_all(cut_along(shard, dim, length), axis, 0, 0, tiled=True)  54.5 us
    all_to_all x1, blocking collectives, local(): lax.all_to_all(outbox, 'ep', split_axis=0, concat_axis=0, tiled=True)  39.5 us
    all_to_all x1, waiting for transfers between devices, local(): lax.all_to_all(sums.astype(jnp.bfloat16), 'ep', split_axis=1, concat_axis...  21.6 us
    all_to_all x1, starting transfers between devices, local(): lax.all_to_all(sums.astype(jnp.bfloat16), 'ep', split_axis=1, concat_axis...  15.5 us
    all_to_all x2, starting transfers between devices, from_everyone(): return lax.all_to_all(copies, axis, split_axis=0, concat_axis=0, tiled=True)  11.1 us
    dot_general x1, matrix products, local(): lax.dot_general(down_w, hidden, (((0,), (1,)), ((), ())), preferred_eleme...  9.6 us
    all_to_all x2, waiting for transfers between devices, from_everyone(): return lax.all_to_all(copies, axis, split_axis=0, concat_axis=0, tiled=True)  8.25 us
  transfers between devices with their start and end apart: 4, of which 4 were waited for; matrix products, arithmetic and copies ran while one was open for 2% of the time, Pallas kernels for 0%

commit v1 on v0

v1 whole, which is shorter than its diff:
```python
import functools

import jax
import jax.numpy as jnp
from jax import lax
from jax.experimental import pallas as pl
from jax.experimental.pallas import tpu as pltpu
from jax.sharding import PartitionSpec as P

EPS = 1e-06
LANES = 128
MESH = pl.DeviceIdType.MESH
BF, F32 = jnp.bfloat16, jnp.float32

ORDERS = (
    (("x", 0), ("y", 0), ("x", 1), ("y", 1)),
    (("y", 0), ("x", 1), ("y", 1), ("x", 0)),
    (("x", 1), ("y", 1), ("x", 0), ("y", 0)),
    (("y", 1), ("x", 0), ("y", 0), ("x", 1)),
)
STAGGER = 3


def block_index(quarter, y, x):
    place = {}
    index = 0
    seen = {"x": 0, "y": 0}
    for bit, (axis, parity) in enumerate(ORDERS[quarter]):
        at = x if axis == "x" else y
        if seen[axis] == 0:
            place[axis] = (at + parity) % 4
            index = index + (place[axis] % 2) * 2**bit
        else:
            index = index + (place[axis] // 2) * 2**bit
        seen[axis] += 1
    return index


def partner(axis, parity, y, x):
    at = x if axis == "x" else y
    step = 1 - 2 * ((at + parity) % 2)
    other = (at + step + 4) % 4
    return y * 4 + other if axis == "x" else other * 4 + x


def distances(chips):
    out = [0]
    for d in range(1, chips // 2 + 1):
        out.append(d)
        if d != chips - d:
            out.append(-d)
    return out


def body(
    chips,
    tok_ref,
    gain_ref,
    routes_ref,
    rw_ref,
    fg_ref,
    wg_hbm,
    wu_hbm,
    wd_hbm,
    out_ref,
    w1,
    wd,
    outbox,
    gather,
    normed,
    parts,
    in0,
    in1,
    in2,
    in3,
    done,
    returned,
    gains,
    squares,
    w_sem,
    disp_send,
    disp_recv,
    ag_send,
    ag_recv,
    rs_send,
    rs_recv,
    ret_send,
    ret_recv,
    gain_send,
    gain_recv,
    sq_send,
    sq_recv,
):
    inbound = (in0, in1, in2, in3)
    ep, tp = lax.axis_index("ep"), lax.axis_index("tp")
    z, core = ep // 2, ep % 2
    y, x = tp // 4, tp % 4
    tokens = tok_ref.shape[0]
    experts, cap = outbox.shape[0], outbox.shape[1]
    items = chips
    rounds = items // 4
    rows = 2 * cap
    width = 16 * LANES
    hidden_units = wd.shape[0]
    dz = distances(chips)

    loads = (
        pltpu.make_async_copy(wg_hbm.at[0], w1.at[:, pl.ds(0, hidden_units)], w_sem.at[0]),
        pltpu.make_async_copy(wu_hbm.at[0], w1.at[:, pl.ds(hidden_units, hidden_units)], w_sem.at[1]),
        pltpu.make_async_copy(wd_hbm.at[0], wd, w_sem.at[2]),
    )
    for load in loads:
        load.start()

    def ahead(item, dc):
        return ((z + dz[item] + chips) % chips) * 2 + (core + dc) % 2

    def behind(item, dc):
        return ((z - dz[item] + chips) % chips) * 2 + (core + dc) % 2

    barrier = pltpu.get_barrier_semaphore()
    far = [(item, dc) for item in range(items) for dc in range(2) if (item, dc) != (0, 0)]
    for item, dc in reversed(far):
        pl.semaphore_signal(barrier, inc=1, device_id=(ahead(item, dc), tp), device_id_type=MESH)
    for off in range(1, 16):
        pl.semaphore_signal(barrier, inc=1, device_id=(ep, (tp + off) % 16), device_id_type=MESH)

    r0 = jnp.broadcast_to(routes_ref[:, 0:1], (tokens, LANES))
    r1 = jnp.broadcast_to(routes_ref[:, 1:2], (tokens, LANES))
    lane = lax.broadcasted_iota(jnp.int32, (tokens, LANES), 1)
    hit0 = jnp.where(r0 == lane, 1.0, 0.0).astype(F32)
    hit1 = jnp.where(r1 == lane, 1.0, 0.0).astype(F32)
    below = jnp.where(
        lax.broadcasted_iota(jnp.int32, (tokens, tokens), 0) > lax.broadcasted_iota(jnp.int32, (tokens, tokens), 1),
        1.0,
        0.0,
    ).astype(BF)
    before = jnp.dot(below, (hit0 + hit1).astype(BF), preferred_element_type=F32)
    target0 = jnp.sum(hit0 * (before + lane.astype(F32) * cap), axis=1, keepdims=True)
    target1 = jnp.sum(hit1 * (before + lane.astype(F32) * cap), axis=1, keepdims=True)
    across0 = jnp.transpose(jnp.broadcast_to(target0, (tokens, LANES)))[0:1, :]
    across1 = jnp.transpose(jnp.broadcast_to(target1, (tokens, LANES)))[0:1, :]
    piece = 256
    for start in range(0, experts * cap, piece):
        slot = (lax.broadcasted_iota(jnp.int32, (piece, tokens), 0) + start).astype(F32)
        pick = jnp.where((slot == across0) | (slot == across1), 1.0, 0.0).astype(BF)
        picked = jnp.dot(pick, tok_ref[...], preferred_element_type=F32).astype(BF)
        outbox[pl.ds(start // cap, piece // cap)] = picked.reshape(piece // cap, cap, LANES)
    gains[pl.ds(tp, 1)] = gain_ref[...].astype(F32).reshape(1, 1, LANES)

    pl.semaphore_wait(barrier, len(far) + 15)

    mine = [block_index(q, y, x) for q in range(4)]
    gather[0, pl.ds(mine[0], 1), pl.ds(0, cap)] = outbox[pl.ds(ep, 1)]

    def dispatch(item, dc):
        return pltpu.make_async_remote_copy(
            src_ref=outbox.at[ahead(item, dc)],
            dst_ref=gather.at[item, mine[item % 4], pl.ds(dc * cap, cap)],
            send_sem=disp_send.at[item, dc],
            recv_sem=disp_recv.at[item, dc],
            device_id=(ahead(item, dc), tp),
            device_id_type=MESH,
        )

    for item, dc in far:
        dispatch(item, dc).start()

    def small(buffer, sends, recvs, off):
        return pltpu.make_async_remote_copy(
            src_ref=buffer.at[tp],
            dst_ref=buffer.at[tp],
            send_sem=sends.at[off],
            recv_sem=recvs.at[off],
            device_id=(ep, (tp + off) % 16),
            device_id_type=MESH,
        )

    for off in range(1, 16):
        small(gains, gain_send, gain_recv, off).start()

    def gather_copy(item, stage):
        axis, parity = ORDERS[item % 4][stage]
        group = pl.ds((mine[item % 4] // 2**stage) * 2**stage, 2**stage)
        return pltpu.make_async_remote_copy(
            src_ref=gather.at[item, group],
            dst_ref=gather.at[item, group],
            send_sem=ag_send.at[item, stage],
            recv_sem=ag_recv.at[item, stage],
            device_id=(ep, partner(axis, parity, y, x)),
            device_id_type=MESH,
        )

    def scatter_copy(item, stage):
        bit = 3 - stage
        axis, parity = ORDERS[item % 4][bit]
        index = mine[item % 4]
        base = (index // 2 ** (bit + 1)) * 2 ** (bit + 1)
        sent = base + (1 - (index // 2**bit) % 2) * 2**bit
        return pltpu.make_async_remote_copy(
            src_ref=parts.at[item, pl.ds(sent, 2**bit)],
            dst_ref=inbound[stage].at[item],
            send_sem=rs_send.at[item, stage],
            recv_sem=rs_recv.at[item, stage],
            device_id=(ep, partner(axis, parity, y, x)),
            device_id_type=MESH,
        )

    def give_back(item, dc):
        return pltpu.make_async_remote_copy(
            src_ref=done.at[item, pl.ds(dc * cap, cap)],
            dst_ref=returned.at[ep],
            send_sem=ret_send.at[item, dc],
            recv_sem=ret_recv.at[item, dc],
            device_id=(behind(item, dc), tp),
            device_id_type=MESH,
        )

    def gather_stage(k, stage):
        for q in range(4):
            item = 4 * k + q
            if stage == 0:
                for dc in range(2):
                    if (item, dc) != (0, 0):
                        dispatch(item, dc).wait_recv()
            else:
                gather_copy(item, stage - 1).wait_recv()
            gather_copy(item, stage).start()

    def experts_stage(k):
        if k == 0:
            for off in range(1, 16):
                small(gains, gain_send, gain_recv, off).wait_recv()
            for load in loads:
                load.wait()
        for q in range(4):
            item = 4 * k + q
            gather_copy(item, 3).wait_recv()
            total = jnp.zeros((rows, LANES), F32)
            for t in range(16):
                row = gather[item, block_index(q, t // 4, t % 4)].astype(F32)
                total = total + row * row
            scale = lax.rsqrt(jnp.sum(total, axis=1, keepdims=True) / width + EPS)
            scale = jnp.broadcast_to(scale, (rows, LANES))
            for t in range(16):
                row = gather[item, block_index(q, t // 4, t % 4)].astype(F32)
                normed[pl.ds(q * rows, rows), pl.ds(t * LANES, LANES)] = (row * scale * gains[t]).astype(BF)
        both = jnp.dot(normed[...], w1[...], preferred_element_type=F32)
        gate, up = both[:, :hidden_units], both[:, hidden_units:]
        hidden = (gate / (1.0 + jnp.exp(-gate)) * up).astype(BF)
        for pair in range(8):
            part = jnp.dot(hidden, wd[:, pl.ds(pair * 256, 256)], preferred_element_type=F32).astype(BF)
            for q in range(4):
                for t in (2 * pair, 2 * pair + 1):
                    parts[4 * k + q, block_index(q, t // 4, t % 4)] = part[
                        q * rows : (q + 1) * rows, (t % 2) * LANES : (t % 2 + 1) * LANES
                    ]
        for q in range(4):
            scatter_copy(4 * k + q, 0).start()

    def scatter_stage(k, stage):
        for q in range(4):
            item = 4 * k + q
            scatter_copy(item, stage - 1).wait_recv()
            bit = 4 - stage
            kept = pl.ds((mine[q] // 2**bit) * 2**bit, 2**bit)
            added = (parts[item, kept].astype(F32) + inbound[stage - 1][item].astype(F32)).astype(BF)
            if stage < 4:
                parts[item, kept] = added
            else:
                done[item] = added[0]
        for q in range(4):
            item = 4 * k + q
            if stage < 4:
                scatter_copy(item, stage).start()
            else:
                for dc in range(2):
                    if (item, dc) == (0, 0):
                        returned[pl.ds(ep, 1)] = done[0, pl.ds(0, cap)].reshape(1, cap, LANES)
                    else:
                        give_back(item, dc).start()

    schedule = []
    for k in range(rounds):
        for s in range(4):
            schedule.append((s + STAGGER * k, k, functools.partial(gather_stage, k, s)))
        schedule.append((4 + STAGGER * k, k, functools.partial(experts_stage, k)))
        for s in range(1, 5):
            schedule.append((4 + s + STAGGER * k, k, functools.partial(scatter_stage, k, s)))
    for _, _, run in sorted(schedule, key=lambda entry: entry[:2]):
        run()

    for item, dc in far:
        give_back(item, dc).wait_recv()
    slot = lax.broadcasted_iota(jnp.int32, (tokens, experts * cap), 1).astype(F32)
    mix = jnp.where(slot == target0, rw_ref[:, 0:1], 0.0) + jnp.where(slot == target1, rw_ref[:, 1:2], 0.0)
    high = mix.astype(BF)
    low = (mix - high.astype(F32)).astype(BF)
    results = returned[...].reshape(experts * cap, LANES)
    combined = jnp.dot(high, results, preferred_element_type=F32) + jnp.dot(low, results, preferred_element_type=F32)

    squares[pl.ds(tp, 1)] = jnp.sum(jnp.transpose(combined * combined), axis=0, keepdims=True).reshape(1, 1, tokens)
    for off in range(1, 16):
        small(squares, sq_send, sq_recv, off).start()
    for off in range(1, 16):
        small(squares, sq_send, sq_recv, off).wait_recv()
    total = squares[0]
    for t in range(1, 16):
        total = total + squares[t]
    final = lax.rsqrt(total / width + EPS)
    final = jnp.transpose(jnp.broadcast_to(final, (LANES, tokens)))
    out_ref[...] = (combined * final * fg_ref[...].astype(F32)).astype(BF)

    for item, dc in far:
        dispatch(item, dc).wait_send()
        give_back(item, dc).wait_send()
    for off in range(1, 16):
        small(gains, gain_send, gain_recv, off).wait_send()
        small(squares, sq_send, sq_recv, off).wait_send()
    for item in range(items):
        for stage in range(4):
            gather_copy(item, stage).wait_send()
            scatter_copy(item, stage).wait_send()


def local(tokens, norm_gain, w_gate, w_up, w_down, routes, route_weights, final_gain):
    experts = lax.axis_size("ep")
    chips = experts // 2
    tok_rows, share = tokens.shape
    cap = 2 * tok_rows * routes.shape[1] // experts
    hidden_units = w_gate.shape[2]
    rows = 2 * cap
    vmem = pl.BlockSpec(memory_space=pltpu.VMEM)
    hbm = pl.BlockSpec(memory_space=pl.ANY)
    dma = pltpu.SemaphoreType.DMA
    return pl.pallas_call(
        functools.partial(body, chips),
        out_shape=jax.ShapeDtypeStruct((tok_rows, share), BF),
        in_specs=[vmem] * 5 + [hbm] * 3,
        out_specs=vmem,
        scratch_shapes=[
            pltpu.VMEM((16 * share, 2 * hidden_units), BF),
            pltpu.VMEM((hidden_units, 16 * share), BF),
            pltpu.VMEM((experts, cap, share), BF),
            pltpu.VMEM((chips, 16, rows, share), BF),
            pltpu.VMEM((4 * rows, 16 * share), BF),
            pltpu.VMEM((chips, 16, rows, share), BF),
            pltpu.VMEM((chips, 8, rows, share), BF),
            pltpu.VMEM((chips, 4, rows, share), BF),
            pltpu.VMEM((chips, 2, rows, share), BF),
            pltpu.VMEM((chips, 1, rows, share), BF),
            pltpu.VMEM((chips, rows, share), BF),
            pltpu.VMEM((experts, cap, share), BF),
            pltpu.VMEM((16, 1, share), F32),
            pltpu.VMEM((16, 1, tok_rows), F32),
            dma((3,)),
            dma((chips, 2)),
            dma((chips, 2)),
            dma((chips, 4)),
            dma((chips, 4)),
            dma((chips, 4)),
            dma((chips, 4)),
            dma((chips, 2)),
            dma((chips, 2)),
            dma((16,)),
            dma((16,)),
            dma((16,)),
            dma((16,)),
        ],
        compiler_params=pltpu.CompilerParams(collective_id=0, has_side_effects=True),
    )(
        tokens,
        norm_gain.reshape(1, -1),
        routes,
        route_weights,
        final_gain.reshape(1, -1),
        w_gate,
        w_up,
        w_down,
    )


def solution(mesh):
    in_specs = (
        P("ep", "tp"),
        P("tp"),
        P("ep", None, "tp"),
        P("ep", None, "tp"),
        P("ep", "tp", None),
        P("ep", None),
        P("ep", None),
        P("tp"),
    )
    out_specs = P("ep", "tp")
    return jax.shard_map(local, mesh=mesh, in_specs=in_specs, out_specs=out_specs, check_vma=False)
```

time: 260 us -> 133 us (0.51)
  Pallas kernels: 0 us -> 128 us
  blocking collectives: 94 us -> 0 us
  waiting for transfers between devices: 89.3 us -> 0 us
  starting transfers between devices: 26.6 us -> 0 us
  matrix products: 15.8 us -> 0 us
  between operations: 13.6 us -> 0.01 us
  other arithmetic: 9.22 us -> 0 us
  local copies, waits for them, and re-layouts: 11.2 us -> 4.4 us
    pallas_call x0 -> x1, Pallas kernels: none -> 128 us  [local(): pl.pallas_call(functools.partial(body, chips), out_shape=jax.ShapeDtypeSt...]
    all_to_all x2 -> x0, blocking collectives: 94 us -> none  [the longest x1 54.5 us: summed_on_arrival(): lax.all_to_all(cut_along(shard, dim, length), axis, 0, 0, tiled=True)]
    all_gather x1 -> x0, waiting for transfers between devices: 59.4 us -> none  [local(): piece = lax.all_gather(inbox, 'tp', axis=1, tiled=True)]
    all_to_all x3 -> x0, waiting for transfers between devices: 29.9 us -> none  [the longest x1 21.6 us: local(): lax.all_to_all(sums.astype(jnp.bfloat16), 'ep', split_axis=1, concat_axis...]
    all_to_all x3 -> x0, starting transfers between devices: 26.6 us -> none  [the longest x1 15.5 us: local(): lax.all_to_all(sums.astype(jnp.bfloat16), 'ep', split_axis=1, concat_axis...]
    dot_general x3 -> x0, matrix products: 15.8 us -> none  [the longest x1 9.6 us: local(): lax.dot_general(down_w, hidden, (((0,), (1,)), ((), ())), preferred_eleme...]
    reduce_sum x6 -> x0, other arithmetic: 4.91 us -> none  [the longest x1 3.53 us: summed_on_arrival(): return jnp.sum(tiles.astype(jnp.float32), axis=0)]
    reshape x3 -> x0, local copies, waits for them, and re-layouts: 3.54 us -> none  [the longest x1 3.26 us: cut_along(): return jnp.moveaxis(shard.reshape(*before, length, -1, *after), dim, 0)]
  transfers between devices with their start and end apart: 4 -> 0, of which waited for: 4 -> 0; matrix products, arithmetic and copies ran while one was open for 2% -> 0% of each run, Pallas kernels for 0% -> 0%
where the time goes in v1:
time: 133 us
  Pallas kernels  128 us (96%)
  local copies, waits for them, and re-layouts  4.4 us (3%)
    pallas_call x1, Pallas kernels, local(): pl.pallas_call(functools.partial(body, chips), out_shape=jax.ShapeDtypeSt...  128 us
    unnamed x3, local copies, waits for them, and re-layouts  4.4 us

profile of v1, /device:TPU:1, one launch (start us, length us, event | category | flops | bytes accessed | tf_op | source)
XLA Modules:
  0.0 132.8 jit_solution(5351717415166379846)
XLA Ops:
  0.0 1.5 %copy.9.routes_ref = s32[256,2]{1,0:T(8,128)} copy(s32[256,2]{0,1:T(2,128)} %param.13) | data formatting | bytes 4096 | tf_op args[5]
  1.5 1.5 %copy.10.rw_ref = f32[256,2]{1,0:T(8,128)} copy(f32[256,2]{0,1:T(2,128)} %param.14) | data formatting | bytes 4096 | tf_op args[6]
  2.9 128.4 %shard_map.82 = bf16[256,128]{1,0:T(8,128)(2,1)} custom-call(bf16[256,128]{1,0:T(8,128)(2,1)} %tok_ref.1, bf16[1,128]{1,0:T(2,128)(2,1)} %bitcast.2, s32[256,2]{1,0:T(8,128)} %copy.9.routes_ref, f32[256,2]{1,0:T(8,128)} %copy.10.rw_ref, bf16[1,128]{1,0:T(2,128)(2,1)} %bitcast.3, bf16[1,2048,384]{2,1,0:T(8,128)(2,1)} %wg_hbm.1, bf16[1,2048,384]{2,1,0:T(8,128)(2,1)} %wu_hbm.1, ...), custom_call_target="tpu_custom_call" | custom-call | tf_op jit(solution)/shard_map/pallas_call | solution.py:336
  131.4 1.5 %copy.12 = bf16[256,128]{1,0:T(8,128)(2,1)} copy(bf16[256,128]{1,0:T(8,128)(2,1)} %shard_map.82) | data formatting | bytes 131072

commit v2 on v1

--- a/solution.py
+++ b/solution.py
@@ -18,7 +18,11 @@
     (("x", 1), ("y", 1), ("x", 0), ("y", 0)),
     (("y", 1), ("x", 0), ("y", 0), ("x", 1)),
 )
-STAGGER = 3
+ORDER = (
+    (0, 0), (1, 0), (0, 1), (1, 1), (0, 2), (2, 0), (3, 0), (1, 2), (2, 1), (3, 1), (0, 3), (2, 2),
+    (3, 2), (1, 3), (3, 3), (2, 3), (1, 4), (3, 4), (2, 4), (0, 4), (3, 5), (2, 5), (1, 5), (3, 6),
+    (0, 5), (2, 6), (1, 6), (3, 7), (0, 6), (2, 7), (1, 7), (3, 8), (0, 7), (2, 8), (1, 8), (0, 8),
+)
 
 
 def block_index(quarter, y, x):
@@ -90,6 +94,9 @@
     gain_recv,
     sq_send,
     sq_recv,
+    high,
+    low,
+    entered,
 ):
     inbound = (in0, in1, in2, in3)
     ep, tp = lax.axis_index("ep"), lax.axis_index("tp")
@@ -119,65 +126,119 @@
         return ((z - dz[item] + chips) % chips) * 2 + (core + dc) % 2
 
     barrier = pltpu.get_barrier_semaphore()
+
+    def along(step, dc):
+        return ((z + step + chips) % chips) * 2 + (core + dc) % 2
+
+    near = [(along(step, dc), tp) for step in (-2, -1, 0, 1, 2) for dc in range(2) if (step, dc) != (0, 0)]
+    near += [(ep, partner(axis, parity, y, x)) for axis, parity in ORDERS[0]]
+    for device in near:
+        pl.semaphore_signal(barrier, inc=1, device_id=device, device_id_type=MESH)
     far = [(item, dc) for item in range(items) for dc in range(2) if (item, dc) != (0, 0)]
-    for item, dc in reversed(far):
-        pl.semaphore_signal(barrier, inc=1, device_id=(ahead(item, dc), tp), device_id_type=MESH)
-    for off in range(1, 16):
-        pl.semaphore_signal(barrier, inc=1, device_id=(ep, (tp + off) % 16), device_id_type=MESH)
-
-    r0 = jnp.broadcast_to(routes_ref[:, 0:1], (tokens, LANES))
-    r1 = jnp.broadcast_to(routes_ref[:, 1:2], (tokens, LANES))
-    lane = lax.broadcasted_iota(jnp.int32, (tokens, LANES), 1)
-    hit0 = jnp.where(r0 == lane, 1.0, 0.0).astype(F32)
-    hit1 = jnp.where(r1 == lane, 1.0, 0.0).astype(F32)
-    below = jnp.where(
-        lax.broadcasted_iota(jnp.int32, (tokens, tokens), 0) > lax.broadcasted_iota(jnp.int32, (tokens, tokens), 1),
+
+    prep = jax.named_scope("prep")
+    prep.__enter__()
+    expert = lax.broadcasted_iota(jnp.int32, (experts, tokens), 0)
+    hit0 = jnp.where(routes_ref[0:1, :] == expert, 1.0, 0.0).astype(F32)
+    hit1 = jnp.where(routes_ref[1:2, :] == expert, 1.0, 0.0).astype(F32)
+    above = jnp.where(
+        lax.broadcasted_iota(jnp.int32, (tokens, tokens), 0) < lax.broadcasted_iota(jnp.int32, (tokens, tokens), 1),
         1.0,
         0.0,
     ).astype(BF)
-    before = jnp.dot(below, (hit0 + hit1).astype(BF), preferred_element_type=F32)
-    target0 = jnp.sum(hit0 * (before + lane.astype(F32) * cap), axis=1, keepdims=True)
-    target1 = jnp.sum(hit1 * (before + lane.astype(F32) * cap), axis=1, keepdims=True)
-    across0 = jnp.transpose(jnp.broadcast_to(target0, (tokens, LANES)))[0:1, :]
-    across1 = jnp.transpose(jnp.broadcast_to(target1, (tokens, LANES)))[0:1, :]
+    before = jnp.dot((hit0 + hit1).astype(BF), above, preferred_element_type=F32)
+    base = before + expert.astype(F32) * cap
+    target0 = jnp.sum(hit0 * base, axis=0, keepdims=True)
+    target1 = jnp.sum(hit1 * base, axis=0, keepdims=True)
     piece = 256
     for start in range(0, experts * cap, piece):
         slot = (lax.broadcasted_iota(jnp.int32, (piece, tokens), 0) + start).astype(F32)
-        pick = jnp.where((slot == across0) | (slot == across1), 1.0, 0.0).astype(BF)
+        pick = jnp.where((slot == target0) | (slot == target1), 1.0, 0.0).astype(BF)
         picked = jnp.dot(pick, tok_ref[...], preferred_element_type=F32).astype(BF)
         outbox[pl.ds(start // cap, piece // cap)] = picked.reshape(piece // cap, cap, LANES)
-    gains[pl.ds(tp, 1)] = gain_ref[...].astype(F32).reshape(1, 1, LANES)
-
-    pl.semaphore_wait(barrier, len(far) + 15)
-
     mine = [block_index(q, y, x) for q in range(4)]
+    gains[pl.ds(mine[0], 1)] = gain_ref[...].astype(F32).reshape(1, 1, LANES)
+    prep.__exit__(None, None, None)
+
+    with jax.named_scope("barrier"):
+        pl.semaphore_wait(barrier, len(near))
+
     gather[0, pl.ds(mine[0], 1), pl.ds(0, cap)] = outbox[pl.ds(ep, 1)]
 
     def dispatch(item, dc):
         return pltpu.make_async_remote_copy(
             src_ref=outbox.at[ahead(item, dc)],
             dst_ref=gather.at[item, mine[item % 4], pl.ds(dc * cap, cap)],
-            send_sem=disp_send.at[item, dc],
-            recv_sem=disp_recv.at[item, dc],
+            send_sem=disp_send,
+            recv_sem=disp_recv.at[item],
             device_id=(ahead(item, dc), tp),
             device_id_type=MESH,
         )
 
-    for item, dc in far:
-        dispatch(item, dc).start()
-
-    def small(buffer, sends, recvs, off):
-        return pltpu.make_async_remote_copy(
-            src_ref=buffer.at[tp],
-            dst_ref=buffer.at[tp],
-            send_sem=sends.at[off],
-            recv_sem=recvs.at[off],
+    def dispatch_round(k):
+        for item, dc in far:
+            if item // 4 == k:
+                dispatch(item, dc).start()
+
+    def tell(level):
+        for way, step in enumerate((-(2**level), 2**level)):
+            pl.semaphore_signal(
+                entered.at[level - 1, way], inc=1, device_id=(along(step, 0), tp), device_id_type=MESH
+            )
+
+    def hear(level):
+        for way in range(2):
+            pl.semaphore_wait(entered.at[level - 1, way], 1)
+
+    dispatch_round(0)
+    tell(1)
+
+    with jax.named_scope("weights"):
+        line = lax.broadcasted_iota(jnp.int32, (LANES, tokens), 0)
+        stacked = jnp.where(line == 0, target0, jnp.where(line == 1, target1, 0.0))
+        stacked = jnp.where(line == 2, rw_ref[0:1, :], jnp.where(line == 3, rw_ref[1:2, :], stacked))
+        columns = jnp.transpose(stacked)
+        slot = lax.broadcasted_iota(jnp.int32, (tokens, experts * cap), 1).astype(F32)
+        mix = jnp.where(slot == columns[:, 0:1], columns[:, 2:3], 0.0)
+        mix = mix + jnp.where(slot == columns[:, 1:2], columns[:, 3:4], 0.0)
+        upper = mix.astype(BF)
+        high[...] = upper
+        low[...] = (mix - upper.astype(F32)).astype(BF)
+    with jax.named_scope("hear1"):
+        hear(1)
+    tell(2)
+
+    dispatch_round(1)
+
+    def later_rounds():
+        hear(2)
+        for k in range(2, rounds):
+            dispatch_round(k)
+
+    def all_of(ref, sem):
+        pltpu.make_async_copy(ref, ref, sem).wait()
+
+    def square_copy(off):
+        return pltpu.make_async_remote_copy(
+            src_ref=squares.at[tp],
+            dst_ref=squares.at[tp],
+            send_sem=sq_send,
+            recv_sem=sq_recv,
             device_id=(ep, (tp + off) % 16),
             device_id_type=MESH,
         )
 
-    for off in range(1, 16):
-        small(gains, gain_send, gain_recv, off).start()
+    def gain_copy(stage):
+        axis, parity = ORDERS[0][stage]
+        group = pl.ds((mine[0] // 2**stage) * 2**stage, 2**stage)
+        return pltpu.make_async_remote_copy(
+            src_ref=gains.at[group],
+            dst_ref=gains.at[group],
+            send_sem=gain_send,
+            recv_sem=gain_recv.at[stage],
+            device_id=(ep, partner(axis, parity, y, x)),
+            device_id_type=MESH,
+        )
 
     def gather_copy(item, stage):
         axis, parity = ORDERS[item % 4][stage]
@@ -185,7 +246,7 @@
         return pltpu.make_async_remote_copy(
             src_ref=gather.at[item, group],
             dst_ref=gather.at[item, group],
-            send_sem=ag_send.at[item, stage],
+            send_sem=ag_send,
             recv_sem=ag_recv.at[item, stage],
             device_id=(ep, partner(axis, parity, y, x)),
             device_id_type=MESH,
@@ -200,7 +261,7 @@
         return pltpu.make_async_remote_copy(
             src_ref=parts.at[item, pl.ds(sent, 2**bit)],
             dst_ref=inbound[stage].at[item],
-            send_sem=rs_send.at[item, stage],
+            send_sem=rs_send,
             recv_sem=rs_recv.at[item, stage],
             device_id=(ep, partner(axis, parity, y, x)),
             device_id_type=MESH,
@@ -210,8 +271,8 @@
         return pltpu.make_async_remote_copy(
             src_ref=done.at[item, pl.ds(dc * cap, cap)],
             dst_ref=returned.at[ep],
-            send_sem=ret_send.at[item, dc],
-            recv_sem=ret_recv.at[item, dc],
+            send_sem=ret_send,
+            recv_sem=ret_recv,
             device_id=(behind(item, dc), tp),
             device_id_type=MESH,
         )
@@ -220,22 +281,28 @@
         for q in range(4):
             item = 4 * k + q
             if stage == 0:
-                for dc in range(2):
-                    if (item, dc) != (0, 0):
-                        dispatch(item, dc).wait_recv()
+                filled = pl.ds(cap, cap) if item == 0 else pl.ds(0, rows)
+                all_of(gather.at[item, 0, filled], disp_recv.at[item])
             else:
                 gather_copy(item, stage - 1).wait_recv()
             gather_copy(item, stage).start()
+        if k == 0:
+            if stage > 0:
+                gain_copy(stage - 1).wait_recv()
+            gain_copy(stage).start()
+
+    first = [k for k, stage in ORDER if stage == 4][0]
 
     def experts_stage(k):
-        if k == 0:
-            for off in range(1, 16):
-                small(gains, gain_send, gain_recv, off).wait_recv()
+        for q in range(4):
+            with jax.named_scope("mwait%d%d" % (k, q)):
+                gather_copy(4 * k + q, 3).wait_recv()
+        if k == first:
+            gain_copy(3).wait_recv()
             for load in loads:
                 load.wait()
         for q in range(4):
             item = 4 * k + q
-            gather_copy(item, 3).wait_recv()
             total = jnp.zeros((rows, LANES), F32)
             for t in range(16):
                 row = gather[item, block_index(q, t // 4, t % 4)].astype(F32)
@@ -244,7 +311,7 @@
             scale = jnp.broadcast_to(scale, (rows, LANES))
             for t in range(16):
                 row = gather[item, block_index(q, t // 4, t % 4)].astype(F32)
-                normed[pl.ds(q * rows, rows), pl.ds(t * LANES, LANES)] = (row * scale * gains[t]).astype(BF)
+                normed[pl.ds(q * rows, rows), pl.ds(t * LANES, LANES)] = (row * scale * gains[block_index(0, t // 4, t % 4)]).astype(BF)
         both = jnp.dot(normed[...], w1[...], preferred_element_type=F32)
         gate, up = both[:, :hidden_units], both[:, hidden_units:]
         hidden = (gate / (1.0 + jnp.exp(-gate)) * up).astype(BF)
@@ -280,30 +347,35 @@
                     else:
                         give_back(item, dc).start()
 
-    schedule = []
-    for k in range(rounds):
-        for s in range(4):
-            schedule.append((s + STAGGER * k, k, functools.partial(gather_stage, k, s)))
-        schedule.append((4 + STAGGER * k, k, functools.partial(experts_stage, k)))
-        for s in range(1, 5):
-            schedule.append((4 + s + STAGGER * k, k, functools.partial(scatter_stage, k, s)))
-    for _, _, run in sorted(schedule, key=lambda entry: entry[:2]):
-        run()
-
-    for item, dc in far:
-        give_back(item, dc).wait_recv()
-    slot = lax.broadcasted_iota(jnp.int32, (tokens, experts * cap), 1).astype(F32)
-    mix = jnp.where(slot == target0, rw_ref[:, 0:1], 0.0) + jnp.where(slot == target1, rw_ref[:, 1:2], 0.0)
-    high = mix.astype(BF)
-    low = (mix - high.astype(F32)).astype(BF)
-    results = returned[...].reshape(experts * cap, LANES)
-    combined = jnp.dot(high, results, preferred_element_type=F32) + jnp.dot(low, results, preferred_element_type=F32)
-
-    squares[pl.ds(tp, 1)] = jnp.sum(jnp.transpose(combined * combined), axis=0, keepdims=True).reshape(1, 1, tokens)
-    for off in range(1, 16):
-        small(squares, sq_send, sq_recv, off).start()
-    for off in range(1, 16):
-        small(squares, sq_send, sq_recv, off).wait_recv()
+    for k, stage in ORDER:
+        with jax.named_scope("r%d_s%d" % (k, stage)):
+            if stage < 4:
+                gather_stage(k, stage)
+            elif stage == 4:
+                experts_stage(k)
+            else:
+                scatter_stage(k, stage - 4)
+        if (k, stage) == (0, 0):
+            with jax.named_scope("later"):
+                later_rounds()
+
+    all_of(outbox.at[pl.ds(0, experts - 1)], disp_send)
+    all_of(gains.at[pl.ds(0, 15)], gain_send)
+    all_of(gather.at[:, pl.ds(0, 15)], ag_send)
+    all_of(parts.at[:, pl.ds(0, 15)], rs_send)
+    with jax.named_scope("retwait"):
+        all_of(returned.at[pl.ds(0, experts - 1)], ret_recv)
+    with jax.named_scope("combine"):
+        results = returned[...].reshape(experts * cap, LANES)
+        combined = jnp.dot(high[...], results, preferred_element_type=F32)
+        combined = combined + jnp.dot(low[...], results, preferred_element_type=F32)
+        square = jnp.sum(jnp.transpose(combined * combined), axis=0, keepdims=True)
+        squares[pl.ds(tp, 1)] = square.reshape(1, 1, tokens)
+        for off in range(1, 16):
+            square_copy(off).start()
+    all_of(outbox.at[pl.ds(0, experts - 1)], ret_send)
+    with jax.named_scope("sqwait"):
+        all_of(squares.at[pl.ds(0, 15)], sq_recv)
     total = squares[0]
     for t in range(1, 16):
         total = total + squares[t]
@@ -311,16 +383,7 @@
     final = jnp.transpose(jnp.broadcast_to(final, (LANES, tokens)))
     out_ref[...] = (combined * final * fg_ref[...].astype(F32)).astype(BF)
 
-    for item, dc in far:
-        dispatch(item, dc).wait_send()
-        give_back(item, dc).wait_send()
-    for off in range(1, 16):
-        small(gains, gain_send, gain_recv, off).wait_send()
-        small(squares, sq_send, sq_recv, off).wait_send()
-    for item in range(items):
-        for stage in range(4):
-            gather_copy(item, stage).wait_send()
-            scatter_copy(item, stage).wait_send()
+    all_of(squares.at[pl.ds(0, 15)], sq_send)
 
 
 def local(tokens, norm_gain, w_gate, w_up, w_down, routes, route_weights, final_gain):
@@ -354,25 +417,28 @@
             pltpu.VMEM((16, 1, share), F32),
             pltpu.VMEM((16, 1, tok_rows), F32),
             dma((3,)),
-            dma((chips, 2)),
-            dma((chips, 2)),
+            dma,
+            dma((chips,)),
+            dma,
             dma((chips, 4)),
+            dma,
             dma((chips, 4)),
-            dma((chips, 4)),
-            dma((chips, 4)),
-            dma((chips, 2)),
-            dma((chips, 2)),
-            dma((16,)),
-            dma((16,)),
-            dma((16,)),
-            dma((16,)),
+            dma,
+            dma,
+            dma,
+            dma((4,)),
+            dma,
+            dma,
+            pltpu.VMEM((tok_rows, experts * cap), BF),
+            pltpu.VMEM((tok_rows, experts * cap), BF),
+            pltpu.SemaphoreType.REGULAR((2, 2)),
         ],
         compiler_params=pltpu.CompilerParams(collective_id=0, has_side_effects=True),
     )(
         tokens,
         norm_gain.reshape(1, -1),
-        routes,
-        route_weights,
+        routes.T,
+        route_weights.T,
         final_gain.reshape(1, -1),
         w_gate,
         w_up,

time: 133 us -> 94.6 us (0.71)
  Pallas kernels: 128 us -> 92.9 us
  local copies, waits for them, and re-layouts: 4.4 us -> 1.47 us
    pallas_call x1, Pallas kernels: 128 us -> 92.9 us  [local(): pl.pallas_call(functools.partial(body, chips), out_shape=jax.ShapeDtypeSt...]
    unnamed x3 -> x1, local copies, waits for them, and re-layouts: 4.4 us -> 1.47 us
where the time goes in v2:
time: 94.6 us; the launch traced here: 94.4 us
  Pallas kernels  92.9 us (98%)
  local copies, waits for them, and re-layouts  1.47 us (2%)
    pallas_call x1, Pallas kernels, local(): pl.pallas_call(functools.partial(body, chips), out_shape=jax.ShapeDtypeSt...  92.9 us

profile of v2, /device:TPU:1, one launch (start us, length us, event | category | flops | bytes accessed | tf_op | source)
XLA Modules:
  0.0 94.4 jit_solution(8187339823036079798)
XLA Ops:
  0.0 92.9 %shard_map.82 = bf16[256,128]{1,0:T(8,128)(2,1)} custom-call(bf16[256,128]{1,0:T(8,128)(2,1)} %tok_ref.1, bf16[1,128]{1,0:T(2,128)(2,1)} %bitcast.6, s32[2,256]{1,0:T(2,128)} %bitcast.4, f32[2,256]{1,0:T(2,128)} %bitcast.5, bf16[1,128]{1,0:T(2,128)(2,1)} %bitcast.7, bf16[1,2048,384]{2,1,0:T(8,128)(2,1)} %wg_hbm.1, bf16[1,2048,384]{2,1,0:T(8,128)(2,1)} %wu_hbm.1, ...), custom_call_target="tpu_custom_call" | custom-call | tf_op jit(solution)/shard_map/pallas_call | solution.py:399
  92.9 1.5 %copy.10 = bf16[256,128]{1,0:T(8,128)(2,1)} copy(bf16[256,128]{1,0:T(8,128)(2,1)} %shard_map.82) | data formatting | bytes 131072

commit v3 on v2

v3 whole, which is shorter than its diff:
```python
import functools

import jax
import jax.numpy as jnp
from jax import lax
from jax.experimental import pallas as pl
from jax.experimental.pallas import tpu as pltpu
from jax.sharding import PartitionSpec as P

EPS = 1e-06
LANES = 128
MESH = pl.DeviceIdType.MESH
BF, F32 = jnp.bfloat16, jnp.float32

ORDERS = (
    (("x", 0), ("y", 0), ("x", 1), ("y", 1)),
    (("y", 0), ("x", 1), ("y", 1), ("x", 0)),
    (("x", 1), ("y", 1), ("x", 0), ("y", 0)),
    (("y", 1), ("x", 0), ("y", 0), ("x", 1)),
)
ORDER = (
    (0, 0), (1, 0), (0, 1), (1, 1), (0, 2), (3, 0), (2, 0), (0, 3), (3, 1), (2, 1), (1, 2), (3, 2),
    (2, 2), (1, 3), (3, 3), (2, 3), (0, 4), (3, 4), (2, 4), (3, 5), (1, 4), (3, 6), (2, 5), (1, 5),
    (3, 7), (2, 6), (0, 5), (1, 6), (3, 8), (2, 7), (0, 6), (1, 7), (2, 8), (0, 7), (1, 8), (0, 8),
)
SOURCES = 2


def block_index(quarter, y, x):
    place = {}
    index = 0
    seen = {"x": 0, "y": 0}
    for bit, (axis, parity) in enumerate(ORDERS[quarter]):
        at = x if axis == "x" else y
        if seen[axis] == 0:
            place[axis] = (at + parity) % 4
            index = index + (place[axis] % 2) * 2**bit
        else:
            index = index + (place[axis] // 2) * 2**bit
        seen[axis] += 1
    return index


def partner(axis, parity, y, x):
    at = x if axis == "x" else y
    step = 1 - 2 * ((at + parity) % 2)
    other = (at + step + 4) % 4
    return (y, other) if axis == "x" else (other, x)


def handed_on(index, bit):
    return (index // 2 ** (bit + 1)) * 2 ** (bit + 1) + (1 - (index // 2**bit) % 2) * 2**bit


def landing(stage, step):
    return 2 ** (3 - stage) - (2 ** (4 - step))


def distances(chips):
    out = [0]
    for d in range(1, chips // 2 + 1):
        out.append(d)
        if d != chips - d:
            out.append(-d)
    return out


def body(
    chips,
    tok_hbm,
    gain_hbm,
    routes_hbm,
    rw_hbm,
    fg_hbm,
    wg_hbm,
    wu_hbm,
    wd_hbm,
    out_ref,
    w1,
    wd,
    outbox,
    gather,
    normed,
    parts,
    in0,
    in1,
    in2,
    in3,
    done,
    returned,
    gains,
    squares,
    w_sem,
    disp_send,
    disp_recv,
    ag_send,
    ag_recv,
    rs_send,
    rs_recv,
    ret_send,
    ret_recv,
    gain_send,
    gain_recv,
    sq_send,
    sq_recv,
    high,
    low,
    entered,
    tok_ref,
    gain_ref,
    routes_ref,
    rw_ref,
    fg_ref,
    op_sem,
):
    inbound = (in0, in1, in2, in3)
    ep, tp = lax.axis_index("ep"), lax.axis_index("tp")
    z, core = ep // 2, ep % 2
    y, x = tp // 4, tp % 4
    tokens = tok_ref.shape[0]
    experts, cap = outbox.shape[0], outbox.shape[1]
    items = experts // SOURCES
    rounds = items // 4
    rows = SOURCES * cap
    width = 16 * LANES
    hidden_units = wd.shape[0]
    dz = distances(chips)

    def ahead(n):
        return ((z + dz[n // 2] + chips) % chips) * 2 + (core + n) % 2

    def behind(n):
        return ((z - dz[n // 2] + chips) % chips) * 2 + (core + n) % 2

    barrier = pltpu.get_barrier_semaphore()

    def along(step, dc):
        return ((z + step + chips) % chips) * 2 + (core + dc) % 2

    near = [(along(step, dc), tp) for step in range(-4, 5) for dc in range(2) if (step, dc) != (0, 0)]
    plane = [[partner(axis, parity, y, x) for axis, parity in ORDERS[q]] for q in range(4)]
    near += [(ep, at[0] * 4 + at[1]) for at in plane[0]]
    for device in near:
        pl.semaphore_signal(barrier, inc=1, device_id=device, device_id_type=MESH)

    small_loads = [
        pltpu.make_async_copy(src, dst, op_sem.at[i])
        for i, (src, dst) in enumerate(
            ((routes_hbm, routes_ref), (tok_hbm, tok_ref), (gain_hbm, gain_ref), (rw_hbm, rw_ref), (fg_hbm, fg_ref))
        )
    ]
    for load in small_loads:
        load.start()
    loads = (
        pltpu.make_async_copy(wg_hbm.at[0], w1.at[:, pl.ds(0, hidden_units)], w_sem.at[0]),
        pltpu.make_async_copy(wu_hbm.at[0], w1.at[:, pl.ds(hidden_units, hidden_units)], w_sem.at[1]),
        pltpu.make_async_copy(wd_hbm.at[0], wd, w_sem.at[2]),
    )
    for load in loads:
        load.start()

    prep = jax.named_scope("prep")
    prep.__enter__()
    for load in small_loads:
        load.wait()
    expert = lax.broadcasted_iota(jnp.int32, (experts, tokens), 0)
    hit0 = jnp.where(routes_ref[0:1, :] == expert, 1.0, 0.0).astype(F32)
    hit1 = jnp.where(routes_ref[1:2, :] == expert, 1.0, 0.0).astype(F32)
    above = jnp.where(
        lax.broadcasted_iota(jnp.int32, (tokens, tokens), 0) < lax.broadcasted_iota(jnp.int32, (tokens, tokens), 1),
        1.0,
        0.0,
    ).astype(BF)
    before = jnp.dot((hit0 + hit1).astype(BF), above, preferred_element_type=F32)
    base = before + expert.astype(F32) * cap
    target0 = jnp.sum(hit0 * base, axis=0, keepdims=True)
    target1 = jnp.sum(hit1 * base, axis=0, keepdims=True)
    piece = 256
    for start in range(0, experts * cap, piece):
        slot = (lax.broadcasted_iota(jnp.int32, (piece, tokens), 0) + start).astype(F32)
        pick = jnp.where((slot == target0) | (slot == target1), 1.0, 0.0).astype(BF)
        picked = jnp.dot(pick, tok_ref[...], preferred_element_type=F32).astype(BF)
        outbox[pl.ds(start // cap, piece // cap)] = picked.reshape(piece // cap, cap, LANES)
    mine = [block_index(q, y, x) for q in range(4)]
    theirs = [[block_index(q, *at) for at in plane[q]] for q in range(4)]
    gains[pl.ds(mine[0], 1)] = gain_ref[...].astype(F32).reshape(1, 1, LANES)
    prep.__exit__(None, None, None)

    with jax.named_scope("barrier"):
        pl.semaphore_wait(barrier, len(near))

    gather[0, pl.ds(mine[0], 1), pl.ds(0, cap)] = outbox[pl.ds(ep, 1)]

    def dispatch(n):
        item = n // SOURCES
        pltpu.make_async_remote_copy(
            src_ref=outbox.at[ahead(n)],
            dst_ref=gather.at[item, mine[item % 4], pl.ds(n % SOURCES * cap, cap)],
            send_sem=disp_send,
            recv_sem=disp_recv.at[item // 4],
            device_id=(ahead(n), tp),
            device_id_type=MESH,
        ).start()

    def dispatch_round(k):
        for n in range(4 * SOURCES * k, 4 * SOURCES * (k + 1)):
            if n > 0:
                dispatch(n)

    close = 4 // SOURCES
    for k in range(close):
        dispatch_round(k)
    for way, step in enumerate((-4, 4)):
        pl.semaphore_signal(entered.at[way], inc=1, device_id=(along(step, 0), tp), device_id_type=MESH)

    with jax.named_scope("weights"):
        line = lax.broadcasted_iota(jnp.int32, (LANES, tokens), 0)
        stacked = jnp.where(line == 0, target0, jnp.where(line == 1, target1, 0.0))
        stacked = jnp.where(line == 2, rw_ref[0:1, :], jnp.where(line == 3, rw_ref[1:2, :], stacked))
        columns = jnp.transpose(stacked)
        slot = lax.broadcasted_iota(jnp.int32, (tokens, experts * cap), 1).astype(F32)
        mix = jnp.where(slot == columns[:, 0:1], columns[:, 2:3], 0.0)
        mix = mix + jnp.where(slot == columns[:, 1:2], columns[:, 3:4], 0.0)
        upper = mix.astype(BF)
        high[...] = upper
        low[...] = (mix - upper.astype(F32)).astype(BF)
    with jax.named_scope("hear"):
        for way in range(2):
            pl.semaphore_wait(entered.at[way], 1)
    for k in range(rounds - 1, close - 1, -1):
        dispatch_round(k)

    def all_of(ref, sem):
        pltpu.make_async_copy(ref, ref, sem).wait()

    def square_copy(off):
        return pltpu.make_async_remote_copy(
            src_ref=squares.at[tp],
            dst_ref=squares.at[tp],
            send_sem=sq_send,
            recv_sem=sq_recv,
            device_id=(ep, (tp + off) % 16),
            device_id_type=MESH,
        )

    def across(q, bit, src, dst, send_sem, recv_sem):
        at = plane[q][bit]
        pltpu.make_async_remote_copy(
            src_ref=src,
            dst_ref=dst,
            send_sem=send_sem,
            recv_sem=recv_sem,
            device_id=(ep, at[0] * 4 + at[1]),
            device_id_type=MESH,
        ).start()

    def gather_stage(k, stage):
        if stage == 0:
            sources = 4 * SOURCES - (1 if k == 0 else 0)
            all_of(outbox.at[pl.ds(0, sources)], disp_recv.at[k])
        for q in range(4):
            item = 4 * k + q
            if stage == 0:
                blocks = gather.at[item, pl.ds(mine[q], 1)]
            else:
                all_of(gather.at[item, pl.ds(0, 2 ** (stage - 1))], ag_recv.at[item, stage - 1])
                blocks = gather.at[item, pl.ds(handed_on(mine[q], stage - 1), 2 ** (stage - 1))]
            for bit in range(stage, 4):
                across(q, bit, blocks, blocks, ag_send, ag_recv.at[item, bit])
        if k == 0:
            if stage > 0:
                all_of(gains.at[pl.ds(0, 2 ** (stage - 1))], gain_recv.at[stage - 1])
            group = gains.at[pl.ds((mine[0] // 2**stage) * 2**stage, 2**stage)]
            across(0, stage, group, group, gain_send, gain_recv.at[stage])

    def scatter_send(item, stage):
        bit = 3 - stage
        q = item % 4
        other = theirs[q][bit]
        for step in range(stage + 1, 5):
            start = landing(stage, step)
            size = 2 ** (3 - step) if step < 4 else 1
            block = handed_on(other, 3 - step) if step < 4 else other
            across(
                q,
                bit,
                parts.at[item, pl.ds(block, size)],
                inbound[stage].at[item, pl.ds(start, size)],
                rs_send,
                rs_recv.at[item, step - 1],
            )

    def give_back(n):
        pltpu.make_async_remote_copy(
            src_ref=done.at[n // SOURCES, pl.ds(n % SOURCES * cap, cap)],
            dst_ref=returned.at[ep],
            send_sem=ret_send,
            recv_sem=ret_recv,
            device_id=(behind(n), tp),
            device_id_type=MESH,
        ).start()

    first = [k for k, stage in ORDER if stage == 4][0]

    def experts_stage(k):
        for q in range(4):
            all_of(gather.at[4 * k + q, pl.ds(0, 8)], ag_recv.at[4 * k + q, 3])
        if k == first:
            all_of(gains.at[pl.ds(0, 8)], gain_recv.at[3])
            for load in loads:
                load.wait()
        for q in range(4):
            item = 4 * k + q
            total = jnp.zeros((rows, LANES), F32)
            for t in range(16):
                row = gather[item, block_index(q, t // 4, t % 4)].astype(F32)
                total = total + row * row
            scale = lax.rsqrt(jnp.sum(total, axis=1, keepdims=True) / width + EPS)
            scale = jnp.broadcast_to(scale, (rows, LANES))
            for t in range(16):
                row = gather[item, block_index(q, t // 4, t % 4)].astype(F32)
                normed[pl.ds(q * rows, rows), pl.ds(t * LANES, LANES)] = (row * scale * gains[block_index(0, t // 4, t % 4)]).astype(BF)
        both = jnp.dot(normed[...], w1[...], preferred_element_type=F32)
        gate, up = both[:, :hidden_units], both[:, hidden_units:]
        hidden = (gate / (1.0 + jnp.exp(-gate)) * up).astype(BF)
        for pair in range(8):
            part = jnp.dot(hidden, wd[:, pl.ds(pair * 256, 256)], preferred_element_type=F32).astype(BF)
            for q in range(4):
                for t in (2 * pair, 2 * pair + 1):
                    parts[4 * k + q, block_index(q, t // 4, t % 4)] = part[
                        q * rows : (q + 1) * rows, (t % 2) * LANES : (t % 2 + 1) * LANES
                    ]
        for q in range(4):
            scatter_send(4 * k + q, 0)

    def scatter_stage(k, step):
        size = 2 ** (3 - step) if step < 4 else 1
        for q in range(4):
            item = 4 * k + q
            all_of(parts.at[item, pl.ds(0, step * size)], rs_recv.at[item, step - 1])
            block = pl.ds(handed_on(mine[q], 3 - step) if step < 4 else mine[q], size)
            added = parts[item, block].astype(F32)
            for stage in range(step):
                start = landing(stage, step)
                added = added + inbound[stage][item, start : start + size].astype(F32)
            if step < 4:
                parts[item, block] = added.astype(BF)
            else:
                done[item] = added[0].astype(BF)
        for q in range(4):
            item = 4 * k + q
            if step < 4:
                scatter_send(item, step)
            else:
                for n in range(SOURCES * item, SOURCES * (item + 1)):
                    if n == 0:
                        returned[pl.ds(ep, 1)] = done[0, pl.ds(0, cap)].reshape(1, cap, LANES)
                    else:
                        give_back(n)

    for k, stage in ORDER:
        with jax.named_scope("r%d_s%d" % (k, stage)):
            if stage < 4:
                gather_stage(k, stage)
            elif stage == 4:
                experts_stage(k)
            else:
                scatter_stage(k, stage - 4)

    all_of(outbox.at[pl.ds(0, experts - 1)], disp_send)
    all_of(gains.at[pl.ds(0, 15)], gain_send)
    all_of(gather.at[:, pl.ds(0, 15)], ag_send)
    all_of(parts.at[:, pl.ds(0, 15)], rs_send)
    with jax.named_scope("retwait"):
        all_of(returned.at[pl.ds(0, experts - 1)], ret_recv)
    with jax.named_scope("combine"):
        results = returned[...].reshape(experts * cap, LANES)
        combined = jnp.dot(high[...], results, preferred_element_type=F32)
        combined = combined + jnp.dot(low[...], results, preferred_element_type=F32)
        square = jnp.sum(jnp.transpose(combined * combined), axis=0, keepdims=True)
        squares[pl.ds(tp, 1)] = square.reshape(1, 1, tokens)
        for off in range(1, 16):
            square_copy(off).start()
    all_of(outbox.at[pl.ds(0, experts - 1)], ret_send)
    with jax.named_scope("sqwait"):
        all_of(squares.at[pl.ds(0, 15)], sq_recv)
    total = squares[0]
    for t in range(1, 16):
        total = total + squares[t]
    final = lax.rsqrt(total / width + EPS)
    final = jnp.transpose(jnp.broadcast_to(final, (LANES, tokens)))
    out_ref[...] = (combined * final * fg_ref[...].astype(F32)).astype(BF)

    all_of(squares.at[pl.ds(0, 15)], sq_send)


def local(tokens, norm_gain, w_gate, w_up, w_down, routes, route_weights, final_gain):
    experts = lax.axis_size("ep")
    chips = experts // 2
    items = experts // SOURCES
    tok_rows, share = tokens.shape
    cap = 2 * tok_rows * routes.shape[1] // experts
    hidden_units = w_gate.shape[2]
    rows = SOURCES * cap
    vmem = pl.BlockSpec(memory_space=pltpu.VMEM)
    hbm = pl.BlockSpec(memory_space=pl.ANY)
    dma = pltpu.SemaphoreType.DMA
    return pl.pallas_call(
        functools.partial(body, chips),
        out_shape=jax.ShapeDtypeStruct((tok_rows, share), BF),
        in_specs=[hbm] * 8,
        out_specs=vmem,
        scratch_shapes=[
            pltpu.VMEM((16 * share, 2 * hidden_units), BF),
            pltpu.VMEM((hidden_units, 16 * share), BF),
            pltpu.VMEM((experts, cap, share), BF),
            pltpu.VMEM((items, 16, rows, share), BF),
            pltpu.VMEM((4 * rows, 16 * share), BF),
            pltpu.VMEM((items, 16, rows, share), BF),
            pltpu.VMEM((items, 8, rows, share), BF),
            pltpu.VMEM((items, 4, rows, share), BF),
            pltpu.VMEM((items, 2, rows, share), BF),
            pltpu.VMEM((items, 1, rows, share), BF),
            pltpu.VMEM((items, rows, share), BF),
            pltpu.VMEM((experts, cap, share), BF),
            pltpu.VMEM((16, 1, share), F32),
            pltpu.VMEM((16, 1, tok_rows), F32),
            dma((3,)),
            dma,
            dma((items // 4,)),
            dma,
            dma((items, 4)),
            dma,
            dma((items, 4)),
            dma,
            dma,
            dma,
            dma((4,)),
            dma,
            dma,
            pltpu.VMEM((tok_rows, experts * cap), BF),
            pltpu.VMEM((tok_rows, experts * cap), BF),
            pltpu.SemaphoreType.REGULAR((2,)),
            pltpu.VMEM((tok_rows, share), BF),
            pltpu.VMEM((1, share), BF),
            pltpu.VMEM((2, tok_rows), jnp.int32),
            pltpu.VMEM((2, tok_rows), F32),
            pltpu.VMEM((1, share), BF),
            dma((5,)),
        ],
        compiler_params=pltpu.CompilerParams(collective_id=0, has_side_effects=True),
    )(
        tokens,
        norm_gain.reshape(1, -1),
        routes.T,
        route_weights.T,
        final_gain.reshape(1, -1),
        w_gate,
        w_up,
        w_down,
    )


def solution(mesh):
    in_specs = (
        P("ep", "tp"),
        P("tp"),
        P("ep", None, "tp"),
        P("ep", None, "tp"),
        P("ep", "tp", None),
        P("ep", None),
        P("ep", None),
        P("tp"),
    )
    out_specs = P("ep", "tp")
    return jax.shard_map(local, mesh=mesh, in_specs=in_specs, out_specs=out_specs, check_vma=False)
```

time: 94.6 us -> 87.7 us (0.927)
  Pallas kernels: 92.9 us -> 86.1 us
    pallas_call x1, Pallas kernels: 92.9 us -> 86.1 us  [local(): pl.pallas_call(functools.partial(body, chips), out_shape=jax.ShapeDtypeSt...]
where the time goes in v3:
time: 87.7 us; the launch traced here: 87.6 us
  Pallas kernels  86.1 us (98%)
  local copies, waits for them, and re-layouts  1.47 us (2%)
    pallas_call x1, Pallas kernels, local(): pl.pallas_call(functools.partial(body, chips), out_shape=jax.ShapeDtypeSt...  86.1 us

profile of v3, /device:TPU:1, one launch (start us, length us, event | category | flops | bytes accessed | tf_op | source)
XLA Modules:
  0.0 87.6 jit_solution(12076085801343079660)
XLA Ops:
  0.0 86.1 %shard_map.82 = bf16[256,128]{1,0:T(8,128)(2,1)} custom-call(bf16[256,128]{1,0:T(8,128)(2,1)} %tok_hbm.1, bf16[1,128]{1,0:T(2,128)(2,1)} %bitcast.6, s32[2,256]{1,0:T(2,128)} %bitcast.4, f32[2,256]{1,0:T(2,128)} %bitcast.5, bf16[1,128]{1,0:T(2,128)(2,1)} %bitcast.7, bf16[1,2048,384]{2,1,0:T(8,128)(2,1)} %wg_hbm.1, bf16[1,2048,384]{2,1,0:T(8,128)(2,1)} %wu_hbm.1, ...), custom_call_target="tpu_custom_call" | custom-call | tf_op jit(solution)/shard_map/pallas_call | solution.py:408
  86.1 1.5 %copy.10 = bf16[256,128]{1,0:T(8,128)(2,1)} copy(bf16[256,128]{1,0:T(8,128)(2,1)} %shard_map.82) | data formatting | bytes 131072

commit v4 on v3

--- a/solution.py
+++ b/solution.py
@@ -202,16 +202,17 @@
             device_id_type=MESH,
         ).start()
 
+    close = 4 // SOURCES
+
     def dispatch_round(k):
-        for n in range(4 * SOURCES * k, 4 * SOURCES * (k + 1)):
+        order = range(4 * SOURCES * k, 4 * SOURCES * (k + 1))
+        for n in order if k < close else reversed(order):
             if n > 0:
                 dispatch(n)
 
-    close = 4 // SOURCES
-    for k in range(close):
-        dispatch_round(k)
     for way, step in enumerate((-4, 4)):
         pl.semaphore_signal(entered.at[way], inc=1, device_id=(along(step, 0), tp), device_id_type=MESH)
+    dispatch_round(0)
 
     with jax.named_scope("weights"):
         line = lax.broadcasted_iota(jnp.int32, (LANES, tokens), 0)
@@ -224,6 +225,8 @@
         upper = mix.astype(BF)
         high[...] = upper
         low[...] = (mix - upper.astype(F32)).astype(BF)
+    for k in range(1, close):
+        dispatch_round(k)
     with jax.named_scope("hear"):
         for way in range(2):
             pl.semaphore_wait(entered.at[way], 1)
@@ -347,7 +350,7 @@
                 parts[item, block] = added.astype(BF)
             else:
                 done[item] = added[0].astype(BF)
-        for q in range(4):
+        for q in range(4) if step < 4 else reversed(range(4)):
             item = 4 * k + q
             if step < 4:
                 scatter_send(item, step)

time: 87.7 us -> 86.5 us (0.986)
  Pallas kernels: 86.1 us -> 84.9 us
    pallas_call x1, Pallas kernels: 86.1 us -> 84.9 us  [local(): pl.pallas_call(functools.partial(body, chips), out_shape=jax.ShapeDtypeSt...]
where the time goes in v4:
time: 86.5 us; the launch traced here: 86.4 us
  Pallas kernels  84.9 us (98%)
  local copies, waits for them, and re-layouts  1.47 us (2%)
    pallas_call x1, Pallas kernels, local(): pl.pallas_call(functools.partial(body, chips), out_shape=jax.ShapeDtypeSt...  84.9 us

profile of v4, /device:TPU:1, one launch (start us, length us, event | category | flops | bytes accessed | tf_op | source)
XLA Modules:
  0.0 86.4 jit_solution(5127244534755434377)
XLA Ops:
  0.0 84.9 %shard_map.82 = bf16[256,128]{1,0:T(8,128)(2,1)} custom-call(bf16[256,128]{1,0:T(8,128)(2,1)} %tok_hbm.1, bf16[1,128]{1,0:T(2,128)(2,1)} %bitcast.6, s32[2,256]{1,0:T(2,128)} %bitcast.4, f32[2,256]{1,0:T(2,128)} %bitcast.5, bf16[1,128]{1,0:T(2,128)(2,1)} %bitcast.7, bf16[1,2048,384]{2,1,0:T(8,128)(2,1)} %wg_hbm.1, bf16[1,2048,384]{2,1,0:T(8,128)(2,1)} %wu_hbm.1, ...), custom_call_target="tpu_custom_call" | custom-call | tf_op jit(solution)/shard_map/pallas_call | solution.py:411
  84.9 1.5 %copy.10 = bf16[256,128]{1,0:T(8,128)(2,1)} copy(bf16[256,128]{1,0:T(8,128)(2,1)} %shard_map.82) | data formatting | bytes 131072
